TPU v7x, 512 devices: a whole 4x4x16 slice. The times are simulated.
512 devices in a mesh: fs: 64 (over z, y), tp: 8 (over x, core).
Axes of the slice: x: 4, y: 4, z: 16, core: 2. Of those that a mesh axis runs over, the one named last changes fastest.
Arguments:
- residual_in: bfloat16 [16384, 2048], P(('fs', 'tp')), may hold values from -6 to 6
- gain_first: float32 [2048], replicated, may hold values from 0.1 to 1.9
- gain_mixer: float32 [2048], replicated, may hold values from 0.1 to 1.9
- gain_second: float32 [2048], replicated, may hold values from 0.1 to 1.9
- gate_weight: float32 [2048, 6144], P('fs', 'tp'), may hold values from -0.125 to 0.125
- gate_scale: float32 [6144], P('tp'), may hold values from 0.3 to 3
- up_weight: float32 [2048, 6144], P('fs', 'tp'), may hold values from -0.125 to 0.125
- up_scale: float32 [6144], P('tp'), may hold values from 0.3 to 3
- down_weight: float32 [6144, 2048], P('tp', 'fs'), may hold values from -0.078125 to 0.078125
- down_scale: float32 [2048], P('fs'), may hold values from 0.3 to 3
- query_weight: float32 [2048, 2048], P('fs', 'tp'), may hold values from -0.125 to 0.125
- query_scale: float32 [2048], P('tp'), may hold values from 0.3 to 3
- key_weight: float32 [2048, 2048], P('fs', 'tp'), may hold values from -0.125 to 0.125
- key_scale: float32 [2048], P('tp'), may hold values from 0.3 to 3
- value_weight: float32 [2048, 2048], P('fs', 'tp'), may hold values from -0.125 to 0.125
- value_scale: float32 [2048], P('tp'), may hold values from 0.3 to 3
- output_weight: float32 [2048, 2048], P('tp', 'fs'), may hold values from -0.125 to 0.125
- output_scale: float32 [2048], P('fs'), may hold values from 0.3 to 3
Outputs:
- residual_out: bfloat16 [16384, 2048], P(('fs', 'tp'))
All inputs are finite; a program needn't handle non-finite values.
Results may differ from a plain program's by a relative error of at most 0.028.
Values may be sent and summed in bfloat16 or wider, within the bound.
No kernel may reach another device: no remote copies, remote signals or barrier semaphores. Data moves between devices by JAX's collectives and lax.ppermute only.
A program may use at most 64 MiB of HBM per device.

v0:
```python
import jax
import jax.numpy as jnp
from jax import lax
from jax.sharding import Mesh
from jax.sharding import PartitionSpec as P

HEADS = 8
HEAD_DIM = 256
BLOCK = 64
FS = ("fs_0", "fs_1")
FS_TP = ("fs_0", "fs_1", "tp")
EPSILON = 1e-06
HEAD_FLOOR = 0.25
ROTARY_BASE = 10000.0
HIGHEST = lax.Precision.HIGHEST


def sent_to_all(x, axis):
    peers = lax.axis_size(axis)
    return lax.all_to_all(jnp.broadcast_to(x[None], (peers, *x.shape)), axis, 0, 0, tiled=True)


def in_order(pieces, dim):
    dims = list(pieces.shape[1:])
    dims[dim] *= pieces.shape[0]
    return jnp.moveaxis(pieces, 0, dim).reshape(dims)


def collect(x, axis, dim):
    pieces = sent_to_all(x, axis)
    return in_order(pieces, dim)


def split_up(x, dim, peers):
    dims = x.shape
    pieces = x.reshape(*dims[:dim], peers, dims[dim] // peers, *dims[dim + 1 :])
    return jnp.moveaxis(pieces, dim, 0)


def sent_and_summed(x, axis, dim):
    pieces = split_up(x, dim, lax.axis_size(axis))
    arrived = lax.all_to_all(pieces, axis, split_axis=0, concat_axis=0, tiled=True)
    return arrived.astype(jnp.float32).sum(axis=0)


def gather_turned(arrays, axis, dims):
    turned = [jnp.moveaxis(a, dim, 0) for a, dim in zip(arrays, dims)]
    widths = [t[0].size for t in turned]
    both = jnp.concatenate([t.reshape(-1, w) for t, w in zip(turned, widths)], axis=1)
    whole = lax.all_gather(both, axis, axis=0, tiled=True)
    pieces = jnp.split(whole, [sum(widths[:k]) for k in range(1, len(widths))], axis=1)
    return tuple(
        (
            jnp.moveaxis(b.reshape(-1, *t.shape[1:]), 0, dim)
            for b, t, dim in zip(pieces, turned, dims)
        )
    )


def side_by_side(arrays, axis, dim, along):
    both = jnp.concatenate(arrays, axis=along)
    whole, at, done = (lax.all_gather(both, axis, axis=dim, tiled=True), 0, [])
    for a in arrays:
        done.append(lax.slice_in_dim(whole, at, at + a.shape[along], axis=along))
        at += a.shape[along]
    return tuple(done)


def gather_axes(x, axes, dim):
    whole = x
    for number in range(len(axes) - 1, -1, -1):
        whole = lax.all_gather(whole, axes[number], axis=dim, tiled=True)
    return whole


def normalize(sequence_rows, gain_vector):
    values = sequence_rows.astype(jnp.float32)
    scaled = values * lax.rsqrt(jnp.mean(values * values, axis=-1, keepdims=True) + EPSILON)
    return (scaled * gain_vector).astype(jnp.bfloat16)


def collect_rows(sequence_rows, gain_vector):
    return collect(normalize(sequence_rows, gain_vector), "tp", 0)


def return_rows(inputs, weight, factor):
    term = jnp.dot(inputs, weight, preferred_element_type=jnp.float32) * factor
    return sent_and_summed(
        lax.optimization_barrier(term.astype(jnp.bfloat16))
        .astype(jnp.float32)
        .astype(jnp.bfloat16),
        "tp",
        0,
    )


def head_rates(first_head, head_count, length):
    head_number = (first_head + jnp.arange(head_count)).astype(jnp.float32)
    return jnp.exp(jnp.log(1.0 / 16.0) + head_number / (HEADS - 1) * jnp.log(4.0 / length))


def rotate(values, positions):
    half_width = values.shape[-1] // 2
    frequency = ROTARY_BASE ** (-jnp.arange(half_width, dtype=jnp.float32) * 2.0 / values.shape[-1])
    angles = positions[:, None] * frequency[None, :]
    cosine = jnp.cos(angles)[:, None, :]
    sine_value = jnp.sin(angles)[:, None, :]
    front_half = values[..., :half_width]
    back_half = values[..., half_width:]
    return jnp.concatenate(
        [
            front_half * cosine - back_half * sine_value,
            back_half * cosine + front_half * sine_value,
        ],
        axis=-1,
    )


def retention(query_pre, key_pre, value_pre, decay_rates):
    length, head_count, head_width = query_pre.shape
    positions = jnp.arange(length, dtype=jnp.float32)
    query_rot = rotate(query_pre, positions).astype(jnp.bfloat16)
    key_rot = rotate(key_pre, positions).astype(jnp.bfloat16)
    value_low = value_pre.astype(jnp.bfloat16)
    blocks = length // BLOCK
    inside = jnp.arange(BLOCK, dtype=jnp.float32)
    distance = inside[:, None] - inside[None, :]
    within = jnp.where(
        distance >= 0, jnp.exp(-decay_rates[:, None, None] * jnp.maximum(distance, 0.0)), 0.0
    ) * head_width ** (-0.5)
    query_blocks = query_rot.reshape(blocks, BLOCK, head_count, head_width)
    key_blocks = key_rot.reshape(blocks, BLOCK, head_count, head_width)
    value_blocks = value_low.reshape(blocks, BLOCK, head_count, head_width)
    scores = jnp.einsum(
        "nihe,njhe->nhij", query_blocks, key_blocks, preferred_element_type=jnp.float32
    )
    weights = (scores * within[None]).astype(jnp.bfloat16)
    inner_part = jnp.einsum(
        "nhij,njhe->nihe", weights, value_blocks, preferred_element_type=jnp.float32
    )
    fading = jnp.exp(-decay_rates[None, :] * (BLOCK - 1.0 - inside[:, None])) * head_width ** (-0.5)
    key_faded = key_blocks.astype(jnp.float32) * fading[None, :, :, None]
    updates = jnp.einsum(
        "njhd,njhe->nhde", key_faded, value_blocks.astype(jnp.float32), precision=HIGHEST
    )
    block_decay = jnp.exp(-decay_rates * BLOCK)

    def advance(memory_state, update):
        return (memory_state * block_decay[:, None, None] + update, memory_state)

    _, before = lax.scan(
        advance, jnp.zeros((head_count, head_width, head_width), jnp.float32), updates
    )
    rising = jnp.exp(-decay_rates[None, :] * (inside[:, None] + 1.0))
    queried = query_blocks.astype(jnp.float32) * rising[None, :, :, None]
    carried_part = jnp.einsum("nihd,nhde->nihe", queried, before, precision=HIGHEST)
    combined = (inner_part + carried_part).reshape(length, head_count, head_width)
    normed = combined * lax.rsqrt(
        jnp.maximum(jnp.mean(combined * combined, axis=-1, keepdims=True), HEAD_FLOOR)
    )
    return normed.astype(jnp.bfloat16).reshape(length, head_count * head_width)


def body(
    residual_in,
    gain_first,
    gain_mixer,
    gain_second,
    gate_weight,
    gate_scale,
    up_weight,
    up_scale,
    down_weight,
    down_scale,
    query_weight,
    query_scale,
    key_weight,
    key_scale,
    value_weight,
    value_scale,
    output_weight,
    output_scale,
):
    gate_part = gate_weight.astype(jnp.bfloat16)
    up_part = up_weight.astype(jnp.bfloat16)
    down_factor, output_factor = gather_turned((down_scale, output_scale), FS, (0, 0))
    first_input = collect_rows(residual_in, gain_first)
    gate_full, up_full = side_by_side((gate_part, up_part), FS, 0, 1)
    gate_pre = jnp.dot(first_input, gate_full, preferred_element_type=jnp.float32)
    up_pre = jnp.dot(first_input, up_full, preferred_element_type=jnp.float32)
    down_full = gather_axes(down_weight.astype(jnp.bfloat16), FS, 1)
    hidden_first = (jax.nn.silu(gate_pre * gate_scale) * (up_pre * up_scale)).astype(jnp.bfloat16)
    mlp_first = return_rows(hidden_first, down_full, down_factor)
    middle = (residual_in.astype(jnp.float32) + 0.5 * mlp_first).astype(jnp.bfloat16)
    mixer_input = collect_rows(middle, gain_mixer)
    local_width = query_weight.shape[1]
    projections = (
        query_weight.astype(jnp.bfloat16),
        key_weight.astype(jnp.bfloat16),
        value_weight.astype(jnp.bfloat16),
    )
    pieces = side_by_side((projections[0], projections[1], projections[2]), FS, 0, 1)
    query_pre, key_pre, value_pre = tuple(
        (
            jnp.dot(mixer_input, pieces[member], preferred_element_type=jnp.float32)
            for member in range(3)
        )
    )
    output_full = gather_axes(output_weight.astype(jnp.bfloat16), FS, 1)
    length = mixer_input.shape[0]
    heads_local = local_width // HEAD_DIM
    decay_rates = head_rates(lax.axis_index("tp") * heads_local, heads_local, length)
    mixed = retention(
        (query_pre * query_scale).reshape(length, heads_local, HEAD_DIM),
        (key_pre * key_scale).reshape(length, heads_local, HEAD_DIM),
        (value_pre * value_scale).reshape(length, heads_local, HEAD_DIM),
        decay_rates,
    )
    mixer_out = return_rows(mixed, output_full, output_factor)
    second = (middle.astype(jnp.float32) + mixer_out).astype(jnp.bfloat16)
    last_input = collect_rows(second, gain_second)
    gate_last = jnp.dot(last_input, gate_full, preferred_element_type=jnp.float32) * gate_scale
    up_last = jnp.dot(last_input, up_full, preferred_element_type=jnp.float32) * up_scale
    hidden_second = (jax.nn.silu(gate_last) * up_last).astype(jnp.bfloat16)
    mlp_second = return_rows(hidden_second, down_full, down_factor)
    return (second.astype(jnp.float32) + 0.5 * mlp_second).astype(jnp.bfloat16)


def solution(mesh):
    split = Mesh(mesh.devices.reshape(16, 4, mesh.shape["tp"]), ("fs_0", "fs_1", "tp"))
    in_specs = (
        P(FS_TP, None),
        P(),
        P(),
        P(),
        P(FS, "tp"),
        P("tp"),
        P(FS, "tp"),
        P("tp"),
        P("tp", FS),
        P(FS),
        P(FS, "tp"),
        P("tp"),
        P(FS, "tp"),
        P("tp"),
        P(FS, "tp"),
        P("tp"),
        P("tp", FS),
        P(FS),
    )
    out_specs = P(FS_TP, None)
    return jax.shard_map(body, mesh=split, in_specs=in_specs, out_specs=out_specs, check_vma=False)
```

profile of v0, /device:TPU:1, one launch (start us, length us, event | category | flops | bytes accessed | tf_op | source)
XLA Modules:
  0.0 524.1 jit_solution(4226606983639578589)
XLA Ops:
  10.0 11.3 %all_gather.22 = bf16[768,128]{0,1:T(8,128)(2,1)} all-gather(bf16[768,32]{0,1:T(8,128)(2,1)S(1)} %convert_element_type.133), channel_id=1, replica_groups=mesh['fs_0'=16,'fs_1'=4,'tp'=8] {'fs_1'}, dimensions={1}, use_global_device_ids=true | all-gather | bytes 245760 | tf_op jit(solution)/shard_map/all_gather | solution.py:72
  24.3 1.0 fusion.58
  26.4 1.2 broadcast_in_dim.15
  27.6 11.8 %all-to-all-start = ((bf16[8,32,2048]{2,1,0:T(8,128)(2,1)}), bf16[8,32,2048]{2,1,0:T(8,128)(2,1)S(1)}, u32[]{:S(2)}, u32[]{:S(2)}) async-start(bf16[8,32,2048]{2,1,0:T(8,128)(2,1)} %broadcast_in_dim.15), calls=%async_computation | async-start | bytes 2097152 | tf_op jit(solution)/shard_map/all_to_all | solution.py:20
  39.4 72.2 %all-gather = f32[64,32,2]{1,2,0:T(2,128)S(1)} all-gather(f32[1,32,2]{1,2,0:T(2,128)S(1)} %maximum_bitcast_fusion), channel_id=1, replica_groups=mesh['fs_0'=16,'fs_1'=4,'tp'=8] {'fs_0','fs_1'}, dimensions={0}, use_global_device_ids=true | all-gather | bytes 16640 | tf_op jit(solution)/shard_map/all_gather | solution.py:50
  111.8 46.5 %all-gather.6.cloned.1.call-done = bf16[2048,1536]{1,0:T(8,128)(2,1)} async-done(((bf16[32,1536]{1,0:T(8,128)(2,1)}), bf16[2048,1536]{1,0:T(8,128)(2,1)}) %all-gather.6.cloned.1.call-update) | async-done | bytes 6291472 | tf_op jit(solution)/shard_map/all_gather | solution.py:62
  158.3 2.9 fusion.11
  161.2 69.2 %all-gather.8.cloned.1.call-done = bf16[768,2048]{0,1:T(8,128)(2,1)} async-done(((bf16[768,128]{0,1:T(8,128)(2,1)}), bf16[768,2048]{0,1:T(8,128)(2,1)}) %all-gather.8.cloned.1.call-update) | async-done | bytes 3145744 | tf_op jit(solution)/shard_map/all_gather | solution.py:72
  230.4 5.0 fusion.8
  235.4 28.7 %all_to_all.30 = bf16[8,32,2048]{2,1,0:T(8,128)(2,1)S(1)} all-to-all(bf16[8,32,2048]{2,1,0:T(8,128)(2,1)S(1)} %bitcast.75), channel_id=1, replica_groups=mesh['fs_0'=16,'fs_1'=4,'tp'=8] {'tp'}, dimensions={0} | all-to-all | bytes 2097152 | tf_op jit(solution)/shard_map/all_to_all | solution.py:42
  264.6 1.1 broadcast_in_dim.16
  265.7 4.5 all-to-all-start.2
  270.2 10.6 %all_gather.26 = bf16[256,128]{0,1:T(8,128)(2,1)} all-gather(bf16[256,32]{0,1:T(8,128)(2,1)S(1)} %convert_element_type.148), channel_id=1, replica_groups=mesh['fs_0'=16,'fs_1'=4,'tp'=8] {'fs_1'}, dimensions={1}, use_global_device_ids=true | all-gather | bytes 81920 | tf_op jit(solution)/shard_map/all_gather | solution.py:72
  281.0 92.5 %all-gather.10.cloned.1.call-done = bf16[2048,768]{1,0:T(8,128)(2,1)} async-done(((bf16[32,768]{1,0:T(8,128)(2,1)}), bf16[2048,768]{1,0:T(8,128)(2,1)}) %all-gather.10.cloned.1.call-update) | async-done | bytes 3145744 | tf_op jit(solution)/shard_map/all_gather | solution.py:62
  373.5 1.7 fusion.35
  375.2 1.7 fusion.36
  377.5 1.7 fusion.37
  381.8 58.0 %all-gather.12.cloned.1.call-done = bf16[256,2048]{0,1:T(8,128)(2,1)} async-done(((bf16[256,128]{0,1:T(8,128)(2,1)}), bf16[256,2048]{0,1:T(8,128)(2,1)}) %all-gather.12.cloned.1.call-update) | async-done | bytes 1048592 | tf_op jit(solution)/shard_map/all_gather | solution.py:72
  439.8 1.7 fusion.10
  441.5 30.0 %all_to_all.31 = bf16[8,32,2048]{2,1,0:T(8,128)(2,1)S(1)} all-to-all(bf16[8,32,2048]{2,1,0:T(8,128)(2,1)S(1)} %bitcast.66), channel_id=1, replica_groups=mesh['fs_0'=16,'fs_1'=4,'tp'=8] {'tp'}, dimensions={0} | all-to-all | bytes 2097152 | tf_op jit(solution)/shard_map/all_to_all | solution.py:42
  472.0 18.4 %all_to_all.32 = bf16[8,32,2048]{2,1,0:T(8,128)(2,1)S(1)} all-to-all(bf16[8,32,2048]{2,1,0:T(8,128)(2,1)S(1)} %broadcast_in_dim.19), channel_id=1, replica_groups=mesh['fs_0'=16,'fs_1'=4,'tp'=8] {'tp'}, dimensions={0} | all-to-all | bytes 2097152 | tf_op jit(solution)/shard_map/all_to_all | solution.py:20
  490.4 2.9 fusion.14
  493.3 5.0 fusion.9
  498.4 18.4 %all_to_all.33 = bf16[8,32,2048]{2,1,0:T(8,128)(2,1)S(1)} all-to-all(bf16[8,32,2048]{2,1,0:T(8,128)(2,1)S(1)} %bitcast.74), channel_id=1, replica_groups=mesh['fs_0'=16,'fs_1'=4,'tp'=8] {'tp'}, dimensions={0} | all-to-all | bytes 2097152 | tf_op jit(solution)/shard_map/all_to_all | solution.py:42
  (80 shorter events, 13.1 us)
Async XLA Ops:
  6.5 32.9 %copy-start.5 = (f32[32]{0:T(128)S(1)}, f32[32]{0:T(128)}, u32[]{:S(2)}) copy-start(f32[32]{0:T(128)} %param.29) | copy-start | bytes 388
  6.5 32.9 %copy-start.4 = (f32[32]{0:T(128)S(1)}, f32[32]{0:T(128)}, u32[]{:S(2)}) copy-start(f32[32]{0:T(128)} %param.37) | copy-start | bytes 388
  6.5 151.7 %copy-start.6 = (f32[768]{0:T(1024)S(1)}, f32[768]{0:T(1024)}, u32[]{:S(2)}) copy-start(f32[768]{0:T(1024)} %param.25) | copy-start | bytes 9220
  6.5 151.7 %all-gather.6.cloned.1.call-start = ((), (), s32[]{:S(2)}) async-start(), calls=%async_computation.6 | async-start | bytes 6389760 | tf_op jit(solution)/shard_map/all_gather | solution.py:62
  9.1 221.3 %all-gather.8.cloned.1.call-start = ((), (), s32[]{:S(2)}) async-start(), calls=%async_computation.7 | async-start | bytes 3342336 | tf_op jit(solution)/shard_map/all_gather | solution.py:72
  21.3 352.2 %all-gather.10.cloned.1.call-start = ((), (), s32[]{:S(2)}) async-start(), calls=%async_computation.8 | async-start | bytes 3194880 | tf_op jit(solution)/shard_map/all_gather | solution.py:62
  27.6 84.2 %all-to-all-start = ((bf16[8,32,2048]{2,1,0:T(8,128)(2,1)}), bf16[8,32,2048]{2,1,0:T(8,128)(2,1)S(1)}, u32[]{:S(2)}, u32[]{:S(2)}) async-start(bf16[8,32,2048]{2,1,0:T(8,128)(2,1)} %broadcast_in_dim.15), calls=%async_computation | async-start | bytes 2097152 | tf_op jit(solution)/shard_map/all_to_all | solution.py:20
  158.3 72.1 %copy-start.7 = (f32[768]{0:T(1024)S(1)}, f32[768]{0:T(1024)}, u32[]{:S(2)}) copy-start(f32[768]{0:T(1024)} %param.27) | copy-start | bytes 9220
  235.4 28.9 %copy-start = (bf16[32,2048]{1,0:T(8,128)(2,1)S(1)}, bf16[32,2048]{1,0:T(8,128)(2,1)}, u32[]{:S(2)}) copy-start(bf16[32,2048]{1,0:T(8,128)(2,1)} %param.20) | copy-start | bytes 393220
  235.4 29.0 %copy-start.2 = (f32[2048]{0:T(1024)S(1)}, f32[2048]{0:T(1024)}, u32[]{:S(2)}) copy-start(f32[2048]{0:T(1024)} %param.22) | copy-start | bytes 24580
  264.1 6.0 %copy-start.1 = (f32[256,32]{0,1:T(8,128)S(1)}, f32[256,32]{0,1:T(8,128)}, u32[]{:S(2)}) copy-start(f32[256,32]{0,1:T(8,128)} %param.36) | copy-start | bytes 98308
  264.1 109.4 %copy-start.8 = (f32[256]{0:T(256)S(1)}, f32[256]{0:T(256)}, u32[]{:S(2)}) copy-start(f32[256]{0:T(256)} %param.33) | copy-start | bytes 3076
  264.6 110.7 %copy-start.9 = (f32[256]{0:T(256)S(1)}, f32[256]{0:T(256)}, u32[]{:S(2)}) copy-start(f32[256]{0:T(256)} %param.31) | copy-start | bytes 3076
  265.7 107.9 %all-to-all-start.2 = ((bf16[8,32,2048]{2,1,0:T(8,128)(2,1)}), bf16[8,32,2048]{2,1,0:T(8,128)(2,1)S(1)}, u32[]{:S(2)}, u32[]{:S(2)}) async-start(bf16[8,32,2048]{2,1,0:T(8,128)(2,1)} %broadcast_in_dim.16), calls=%async_computation.2 | async-start | bytes 2097152 | tf_op jit(solution)/shard_map/all_to_all | solution.py:20
  270.2 169.6 %all-gather.12.cloned.1.call-start = ((), (), s32[]{:S(2)}) async-start(), calls=%async_computation.9 | async-start | bytes 1114112 | tf_op jit(solution)/shard_map/all_gather | solution.py:72
  280.9 96.5 %copy-start.10 = (f32[256]{0:T(256)S(1)}, f32[256]{0:T(256)}, u32[]{:S(2)}) copy-start(f32[256]{0:T(256)} %param.35) | copy-start | bytes 3076
  381.8 90.0 %copy-start.3 = (f32[2048]{0:T(1024)S(1)}, f32[2048]{0:T(1024)}, u32[]{:S(2)}) copy-start(f32[2048]{0:T(1024)} %param.23) | copy-start | bytes 24580
Sparse Core Ops, SparseCore 0:
  10.3 147.9 all-gather.5
  160.4 69.9 all-gather.7
  233.3 140.1 all-gather.9
  375.5 64.2 all-gather.11
where the time goes:
time: 525 us; the launch traced here: 524 us
  waiting for transfers between devices  266 us (51%)
  blocking collectives  190 us (36%)
  matrix products  24.4 us (5%)
  starting transfers between devices  16.4 us (3%)
  between operations  13.5 us (3%)
  other arithmetic  11.2 us (2%)
    all_gather x2, waiting for transfers between devices, side_by_side(): whole, at, done = (lax.all_gather(both, axis, axis=dim, tiled=True), 0, [])  139 us
    all_gather x2, waiting for transfers between devices, gather_axes(): whole = lax.all_gather(whole, axes[number], axis=dim, tiled=True)  127 us
    all_to_all x3, blocking collectives, sent_and_summed(): lax.all_to_all(pieces, axis, split_axis=0, concat_axis=0, tiled=True)  77.1 us
    all_gather x1, blocking collectives, gather_turned(): whole = lax.all_gather(both, axis, axis=0, tiled=True)  72.2 us
    all_gather x2, blocking collectives, gather_axes(): whole = lax.all_gather(whole, axes[number], axis=dim, tiled=True)  21.9 us
    all_to_all x1, blocking collectives, sent_to_all(): lax.all_to_all(jnp.broadcast_to(x[None], (peers, *x.shape)), axis, 0, 0,...  18.4 us
    all_to_all x2, starting transfers between devices, sent_to_all(): lax.all_to_all(jnp.broadcast_to(x[None], (peers, *x.shape)), axis, 0, 0,...  16.3 us
    dot_general x3, matrix products, return_rows(): term = jnp.dot(inputs, weight, preferred_element_type=jnp.float32) * factor  11.7 us
  transfers between devices with their start and end apart: 6, of which 4 were waited for; matrix products, arithmetic and copies ran while one was open for 5% of the time, Pallas kernels for 0%

commit v1 on v0

--- a/solution.py
+++ b/solution.py
@@ -47,7 +47,9 @@
     turned = [jnp.moveaxis(a, dim, 0) for a, dim in zip(arrays, dims)]
     widths = [t[0].size for t in turned]
     both = jnp.concatenate([t.reshape(-1, w) for t, w in zip(turned, widths)], axis=1)
-    whole = lax.all_gather(both, axis, axis=0, tiled=True)
+    whole = jnp.concatenate(
+        lax.all_to_all(jnp.stack([both] * lax.axis_size(axis)), axis, 0, 0), axis=0
+    )
     pieces = jnp.split(whole, [sum(widths[:k]) for k in range(1, len(widths))], axis=1)
     return tuple(
         (

time: 525 us -> 525 us (level)
  blocking collectives: 190 us -> 117 us
  waiting for transfers between devices: 266 us -> 322 us
  starting transfers between devices: 16.4 us -> 31.5 us
    all_gather x1 -> x0, blocking collectives: 72.2 us -> none  [gather_turned(): whole = lax.all_gather(both, axis, axis=0, tiled=True)]
    all_gather x2, waiting for transfers between devices: 139 us -> 168 us  [side_by_side(): whole, at, done = (lax.all_gather(both, axis, axis=dim, tiled=True), 0, [])]
    all_to_all x0 -> x1, starting transfers between devices: none -> 17.8 us  [gather_turned(): lax.all_to_all(jnp.stack([both] * lax.axis_size(axis)), axis, 0, 0)]
    all_to_all x2, waiting for transfers between devices: 0.01 us -> 14.8 us  [sent_to_all(): lax.all_to_all(jnp.broadcast_to(x[None], (peers, *x.shape)), axis, 0, 0,...]
    all_to_all x0 -> x1, waiting for transfers between devices: none -> 12.6 us  [gather_turned(): lax.all_to_all(jnp.stack([both] * lax.axis_size(axis)), axis, 0, 0)]
  transfers between devices with their start and end apart: 6 -> 7, of which waited for: 4 -> 6; matrix products, arithmetic and copies ran while one was open for 5% -> 5% of each run, Pallas kernels for 0% -> 0%
where the time goes in v1:
time: 525 us; the launch traced here: 524 us
  waiting for transfers between devices  322 us (61%)
  blocking collectives  117 us (22%)
  starting transfers between devices  31.5 us (6%)
  matrix products  24.4 us (5%)
  between operations  13.5 us (3%)
  other arithmetic  11.8 us (2%)
    all_gather x2, waiting for transfers between devices, side_by_side(): whole, at, done = (lax.all_gather(both, axis, axis=dim, tiled=True), 0, [])  168 us
    all_gather x2, waiting for transfers between devices, gather_axes(): whole = lax.all_gather(whole, axes[number], axis=dim, tiled=True)  127 us
    all_to_all x3, blocking collectives, sent_and_summed(): lax.all_to_all(pieces, axis, split_axis=0, concat_axis=0, tiled=True)  77.1 us
    all_gather x2, blocking collectives, gather_axes(): whole = lax.all_gather(whole, axes[number], axis=dim, tiled=True)  21.9 us
    all_to_all x1, blocking collectives, sent_to_all(): lax.all_to_all(jnp.broadcast_to(x[None], (peers, *x.shape)), axis, 0, 0,...  18.4 us
    all_to_all x1, starting transfers between devices, gather_turned(): lax.all_to_all(jnp.stack([both] * lax.axis_size(axis)), axis, 0, 0)  17.8 us
    all_to_all x2, waiting for transfers between devices, sent_to_all(): lax.all_to_all(jnp.broadcast_to(x[None], (peers, *x.shape)), axis, 0, 0,...  14.8 us
    all_to_all x2, starting transfers between devices, sent_to_all(): lax.all_to_all(jnp.broadcast_to(x[None], (peers, *x.shape)), axis, 0, 0,...  13.7 us
  transfers between devices with their start and end apart: 7, of which 6 were waited for; matrix products, arithmetic and copies ran while one was open for 5% of the time, Pallas kernels for 0%

profile of v1, /device:TPU:1, one launch (start us, length us, event | category | flops | bytes accessed | tf_op | source)
XLA Modules:
  0.0 524.3 jit_solution(15250793743828293477)
XLA Ops:
  10.0 11.3 %all_gather.19 = bf16[768,128]{0,1:T(8,128)(2,1)} all-gather(bf16[768,32]{0,1:T(8,128)(2,1)S(1)} %convert_element_type.133), channel_id=1, replica_groups=mesh['fs_0'=16,'fs_1'=4,'tp'=8] {'fs_1'}, dimensions={1}, use_global_device_ids=true | all-gather | bytes 245760 | tf_op jit(solution)/shard_map/all_gather | solution.py:74
  25.6 17.8 %all-to-all-start.1 = ((f32[64,32,2]{1,2,0:T(2,128)}), f32[64,32,2]{1,2,0:T(2,128)S(1)}, u32[]{:S(2)}, u32[]{:S(2)}) async-start(f32[64,32,2]{1,2,0:T(2,128)} %stack.2), calls=%async_computation.1 | async-start | bytes 131072 | tf_op jit(solution)/shard_map/all_to_all | solution.py:51
  45.4 12.6 %all-to-all-done.1 = f32[64,32,2]{1,2,0:T(2,128)S(1)} async-done(((f32[64,32,2]{1,2,0:T(2,128)}), f32[64,32,2]{1,2,0:T(2,128)S(1)}, u32[]{:S(2)}, u32[]{:S(2)}) %all-to-all-start.1) | async-done | bytes 16416 | tf_op jit(solution)/shard_map/all_to_all | solution.py:51
  58.1 1.2 broadcast_in_dim.15
  59.3 9.2 %all-to-all-start = ((bf16[8,32,2048]{2,1,0:T(8,128)(2,1)}), bf16[8,32,2048]{2,1,0:T(8,128)(2,1)S(1)}, u32[]{:S(2)}, u32[]{:S(2)}) async-start(bf16[8,32,2048]{2,1,0:T(8,128)(2,1)} %broadcast_in_dim.15), calls=%async_computation | async-start | bytes 2097152 | tf_op jit(solution)/shard_map/all_to_all | solution.py:20
  68.6 14.8 %all-to-all-done = bf16[8,32,2048]{2,1,0:T(8,128)(2,1)S(1)} async-done(((bf16[8,32,2048]{2,1,0:T(8,128)(2,1)}), bf16[8,32,2048]{2,1,0:T(8,128)(2,1)S(1)}, u32[]{:S(2)}, u32[]{:S(2)}) %all-to-all-start) | async-done | bytes 1048608 | tf_op jit(solution)/shard_map/all_to_all | solution.py:20
  83.4 75.1 %all-gather.5.cloned.1.call-done = bf16[2048,1536]{1,0:T(8,128)(2,1)} async-done(((bf16[32,1536]{1,0:T(8,128)(2,1)}), bf16[2048,1536]{1,0:T(8,128)(2,1)}) %all-gather.5.cloned.1.call-update) | async-done | bytes 6291472 | tf_op jit(solution)/shard_map/all_gather | solution.py:64
  158.5 2.9 fusion.11
  161.4 69.1 %all-gather.7.cloned.1.call-done = bf16[768,2048]{0,1:T(8,128)(2,1)} async-done(((bf16[768,128]{0,1:T(8,128)(2,1)}), bf16[768,2048]{0,1:T(8,128)(2,1)}) %all-gather.7.cloned.1.call-update) | async-done | bytes 3145744 | tf_op jit(solution)/shard_map/all_gather | solution.py:74
  230.5 5.0 fusion.8
  235.6 28.7 %all_to_all.35 = bf16[8,32,2048]{2,1,0:T(8,128)(2,1)S(1)} all-to-all(bf16[8,32,2048]{2,1,0:T(8,128)(2,1)S(1)} %bitcast.73), channel_id=1, replica_groups=mesh['fs_0'=16,'fs_1'=4,'tp'=8] {'tp'}, dimensions={0} | all-to-all | bytes 2097152 | tf_op jit(solution)/shard_map/all_to_all | solution.py:42
  265.8 4.5 all-to-all-start.3
  270.3 10.6 %all_gather.22 = bf16[256,128]{0,1:T(8,128)(2,1)} all-gather(bf16[256,32]{0,1:T(8,128)(2,1)S(1)} %convert_element_type.148), channel_id=1, replica_groups=mesh['fs_0'=16,'fs_1'=4,'tp'=8] {'fs_1'}, dimensions={1}, use_global_device_ids=true | all-gather | bytes 81920 | tf_op jit(solution)/shard_map/all_gather | solution.py:74
  281.2 92.5 %all-gather.9.cloned.1.call-done = bf16[2048,768]{1,0:T(8,128)(2,1)} async-done(((bf16[32,768]{1,0:T(8,128)(2,1)}), bf16[2048,768]{1,0:T(8,128)(2,1)}) %all-gather.9.cloned.1.call-update) | async-done | bytes 3145744 | tf_op jit(solution)/shard_map/all_gather | solution.py:64
  373.7 1.7 fusion.35
  375.4 1.7 fusion.36
  377.7 1.7 fusion.37
  382.0 58.0 %all-gather.11.cloned.1.call-done = bf16[256,2048]{0,1:T(8,128)(2,1)} async-done(((bf16[256,128]{0,1:T(8,128)(2,1)}), bf16[256,2048]{0,1:T(8,128)(2,1)}) %all-gather.11.cloned.1.call-update) | async-done | bytes 1048592 | tf_op jit(solution)/shard_map/all_gather | solution.py:74
  440.0 1.7 fusion.10
  441.7 30.0 %all_to_all.36 = bf16[8,32,2048]{2,1,0:T(8,128)(2,1)S(1)} all-to-all(bf16[8,32,2048]{2,1,0:T(8,128)(2,1)S(1)} %bitcast.64), channel_id=1, replica_groups=mesh['fs_0'=16,'fs_1'=4,'tp'=8] {'tp'}, dimensions={0} | all-to-all | bytes 2097152 | tf_op jit(solution)/shard_map/all_to_all | solution.py:42
  472.2 18.4 %all_to_all.37 = bf16[8,32,2048]{2,1,0:T(8,128)(2,1)S(1)} all-to-all(bf16[8,32,2048]{2,1,0:T(8,128)(2,1)S(1)} %broadcast_in_dim.19), channel_id=1, replica_groups=mesh['fs_0'=16,'fs_1'=4,'tp'=8] {'tp'}, dimensions={0} | all-to-all | bytes 2097152 | tf_op jit(solution)/shard_map/all_to_all | solution.py:20
  490.6 2.9 fusion.14
  493.5 5.0 fusion.9
  498.5 18.4 %all_to_all.38 = bf16[8,32,2048]{2,1,0:T(8,128)(2,1)S(1)} all-to-all(bf16[8,32,2048]{2,1,0:T(8,128)(2,1)S(1)} %bitcast.72), channel_id=1, replica_groups=mesh['fs_0'=16,'fs_1'=4,'tp'=8] {'tp'}, dimensions={0} | all-to-all | bytes 2097152 | tf_op jit(solution)/shard_map/all_to_all | solution.py:42
  (78 shorter events, 16.5 us)
Async XLA Ops:
  6.5 151.9 %copy-start.4 = (f32[768]{0:T(1024)S(1)}, f32[768]{0:T(1024)}, u32[]{:S(2)}) copy-start(f32[768]{0:T(1024)} %param.25) | copy-start | bytes 9220
  6.5 151.9 %all-gather.5.cloned.1.call-start = ((), (), s32[]{:S(2)}) async-start(), calls=%async_computation.7 | async-start | bytes 6389760 | tf_op jit(solution)/shard_map/all_gather | solution.py:64
  9.0 221.5 %all-gather.7.cloned.1.call-start = ((), (), s32[]{:S(2)}) async-start(), calls=%async_computation.8 | async-start | bytes 3342336 | tf_op jit(solution)/shard_map/all_gather | solution.py:74
  21.3 352.4 %all-gather.9.cloned.1.call-start = ((), (), s32[]{:S(2)}) async-start(), calls=%async_computation.9 | async-start | bytes 3194880 | tf_op jit(solution)/shard_map/all_gather | solution.py:64
  25.6 32.5 %all-to-all-start.1 = ((f32[64,32,2]{1,2,0:T(2,128)}), f32[64,32,2]{1,2,0:T(2,128)S(1)}, u32[]{:S(2)}, u32[]{:S(2)}) async-start(f32[64,32,2]{1,2,0:T(2,128)} %stack.2), calls=%async_computation.1 | async-start | bytes 131072 | tf_op jit(solution)/shard_map/all_to_all | solution.py:51
  59.3 24.1 %all-to-all-start = ((bf16[8,32,2048]{2,1,0:T(8,128)(2,1)}), bf16[8,32,2048]{2,1,0:T(8,128)(2,1)S(1)}, u32[]{:S(2)}, u32[]{:S(2)}) async-start(bf16[8,32,2048]{2,1,0:T(8,128)(2,1)} %broadcast_in_dim.15), calls=%async_computation | async-start | bytes 2097152 | tf_op jit(solution)/shard_map/all_to_all | solution.py:20
  158.5 72.1 %copy-start.5 = (f32[768]{0:T(1024)S(1)}, f32[768]{0:T(1024)}, u32[]{:S(2)}) copy-start(f32[768]{0:T(1024)} %param.27) | copy-start | bytes 9220
  235.6 28.9 %copy-start = (bf16[32,2048]{1,0:T(8,128)(2,1)S(1)}, bf16[32,2048]{1,0:T(8,128)(2,1)}, u32[]{:S(2)}) copy-start(bf16[32,2048]{1,0:T(8,128)(2,1)} %param.20) | copy-start | bytes 393220
  235.6 29.0 %copy-start.2 = (f32[2048]{0:T(1024)S(1)}, f32[2048]{0:T(1024)}, u32[]{:S(2)}) copy-start(f32[2048]{0:T(1024)} %param.22) | copy-start | bytes 24580
  264.3 6.0 %copy-start.1 = (f32[256,32]{0,1:T(8,128)S(1)}, f32[256,32]{0,1:T(8,128)}, u32[]{:S(2)}) copy-start(f32[256,32]{0,1:T(8,128)} %param.36) | copy-start | bytes 98308
  264.3 109.4 %copy-start.6 = (f32[256]{0:T(256)S(1)}, f32[256]{0:T(256)}, u32[]{:S(2)}) copy-start(f32[256]{0:T(256)} %param.33) | copy-start | bytes 3076
  264.7 110.7 %copy-start.7 = (f32[256]{0:T(256)S(1)}, f32[256]{0:T(256)}, u32[]{:S(2)}) copy-start(f32[256]{0:T(256)} %param.31) | copy-start | bytes 3076
  265.8 107.9 %all-to-all-start.3 = ((bf16[8,32,2048]{2,1,0:T(8,128)(2,1)}), bf16[8,32,2048]{2,1,0:T(8,128)(2,1)S(1)}, u32[]{:S(2)}, u32[]{:S(2)}) async-start(bf16[8,32,2048]{2,1,0:T(8,128)(2,1)} %broadcast_in_dim.16), calls=%async_computation.3 | async-start | bytes 2097152 | tf_op jit(solution)/shard_map/all_to_all | solution.py:20
  270.3 169.6 %all-gather.11.cloned.1.call-start = ((), (), s32[]{:S(2)}) async-start(), calls=%async_computation.10 | async-start | bytes 1114112 | tf_op jit(solution)/shard_map/all_gather | solution.py:74
  281.1 96.5 %copy-start.8 = (f32[256]{0:T(256)S(1)}, f32[256]{0:T(256)}, u32[]{:S(2)}) copy-start(f32[256]{0:T(256)} %param.35) | copy-start | bytes 3076
  382.0 90.0 %copy-start.3 = (f32[2048]{0:T(1024)S(1)}, f32[2048]{0:T(1024)}, u32[]{:S(2)}) copy-start(f32[2048]{0:T(1024)} %param.23) | copy-start | bytes 24580
Sparse Core Ops, SparseCore 0:
  10.3 148.1 all-gather.4
  160.6 69.9 all-gather.6
  233.5 140.1 all-gather.8
  375.6 64.2 all-gather.10
